TPU v7x, 32 devices: a whole 2x2x4 slice. The times are simulated.
32 devices in a mesh: sp: 8 (over z, x), dp: 4 (over y, core).
Axes of the slice: x: 2, y: 2, z: 4, core: 2. Of those that a mesh axis runs over, the one named last changes fastest.
Arguments:
- normed_input: bfloat16 [2560, 2048], P('sp'), may hold values from -6 to 6
- out_grad: bfloat16 [2560, 2048], P('sp'), may hold values from -6 to 6
- value_weight: bfloat16 [2048, 1024], P(None, 'dp'), may hold values from -0.125 to 0.125
- gate_weight: bfloat16 [2048, 1024], P(None, 'dp'), may hold values from -0.125 to 0.125
- down_weight: bfloat16 [1024, 2048], P('dp'), may hold values from -0.1875 to 0.1875
- conv_kernel: float32 [31, 1024], P(None, 'dp'), may hold values from -5 to 5
- conv_bias: float32 [1024], P('dp'), may hold values from -3 to 3
- norm_gain: float32 [1024], P('dp'), may hold values from 0.1 to 1.9
- norm_shift: float32 [1024], P('dp'), may hold values from -3 to 3
Outputs:
- input_grad: bfloat16 [2560, 2048], P('sp')
- value_grad: float32 [2048, 1024], P('sp', 'dp')
- gate_grad: float32 [2048, 1024], P('sp', 'dp')
- down_grad: float32 [1024, 2048], P('dp', 'sp')
- kernel_grad: float32 [31, 1024], P(None, 'dp')
- bias_grad: float32 [1024], P('dp')
- gain_grad: float32 [1024], P('dp')
- shift_grad: float32 [1024], P('dp')
All inputs are finite; a program needn't handle non-finite values.
Results may differ from a plain program's by a relative error of at most 0.006.
Values may be sent and summed in bfloat16 or wider, within the bound.
A program may use at most 64 MiB of HBM per device.

v0:
```python
import math

import jax
import jax.numpy as jnp
from jax import lax
from jax.sharding import PartitionSpec as P

EPS = 1e-05


def with_halo(block, sides, width):
    for axis, dim in sides:
        count = lax.axis_size(axis)
        forward = [(i, i + 1) for i in range(count - 1)]
        backward = [(target, source) for source, target in forward]
        low = lax.ppermute(
            lax.slice_in_dim(block, block.shape[dim] - width, None, axis=dim), axis, forward
        )
        high = lax.ppermute(lax.slice_in_dim(block, 0, width, axis=dim), axis, backward)
        block = jnp.concatenate([low, block, high], axis=dim)
    return block


def project(weight, rows):
    return lax.dot_general(
        weight, rows, (((0,), (1,)), ((), ())), preferred_element_type=jnp.float32
    )


def on_device(
    normed_input,
    out_grad,
    value_weight,
    gate_weight,
    down_weight,
    conv_kernel,
    conv_bias,
    norm_gain,
    norm_shift,
):
    tokens = normed_input.shape[0]
    width = conv_kernel.shape[0]
    reach = width // 2
    local_channels = value_weight.shape[1]
    channels = local_channels * lax.axis_size("dp")
    ratio = 1.0 / math.sqrt(tokens * lax.axis_size("sp"))
    value_b = project(value_weight, normed_input).astype(jnp.bfloat16)
    gate_b = project(gate_weight, normed_input).astype(jnp.bfloat16)
    value = lax.optimization_barrier(value_b).astype(jnp.float32)
    gate = lax.optimization_barrier(gate_b).astype(jnp.float32)
    opening = jax.nn.sigmoid(gate)
    glu = value * opening
    padded = with_halo(glu, (("sp", 1),), reach)
    mixed = jnp.zeros_like(glu) + conv_bias[:, None]
    for tap in range(width):
        mixed = mixed + conv_kernel[tap][:, None] * padded[:, tap : tap + tokens]
    total, squares = lax.psum((jnp.sum(mixed, axis=0), jnp.sum(mixed * mixed, axis=0)), "dp")
    mean = total / channels
    spread = squares / channels - mean * mean
    inv_std = lax.rsqrt(spread + EPS)
    centred = (mixed - mean[None, :]) * inv_std[None, :]
    normed = centred * norm_gain[:, None] + norm_shift[:, None]
    sig = jax.nn.sigmoid(normed)
    activated = (normed * sig).astype(jnp.bfloat16)
    d_act = lax.dot_general(
        down_weight, out_grad, (((1,), (1,)), ((), ())), preferred_element_type=jnp.float32
    )
    d_normed = d_act * sig * (1.0 + normed * (1.0 - sig))
    d_centred = d_normed * norm_gain[:, None]
    first, second = lax.psum(
        (jnp.sum(d_centred, axis=0), jnp.sum(d_centred * centred, axis=0)), "dp"
    )
    d_mixed = inv_std[None, :] * (
        d_centred - first[None, :] / channels - centred * (second[None, :] / channels)
    )
    d_padded = with_halo(d_mixed, (("sp", 1),), reach)
    d_glu = jnp.zeros_like(d_mixed)
    for tap in range(width):
        d_glu = (
            d_glu
            + conv_kernel[tap][:, None] * d_padded[:, 2 * reach - tap : 2 * reach - tap + tokens]
        )
    kernel_local = jnp.stack(
        [jnp.sum(d_mixed * padded[:, tap : tap + tokens], axis=1) for tap in range(width)]
    )
    kernel_grad, bias_grad, gain_grad, shift_grad = lax.psum(
        (
            kernel_local * ratio,
            jnp.sum(d_mixed, axis=1) * ratio,
            jnp.sum(d_normed * centred, axis=1) * ratio,
            jnp.sum(d_normed, axis=1) * ratio,
        ),
        "sp",
    )
    d_value = (d_glu * opening).astype(jnp.bfloat16)
    d_gate = (d_glu * value * opening * (1.0 - opening)).astype(jnp.bfloat16)
    numbers = (((0,), (1,)), ((), ()))
    value_part = lax.dot_general(normed_input, d_value, numbers, preferred_element_type=jnp.float32)
    gate_part = lax.dot_general(normed_input, d_gate, numbers, preferred_element_type=jnp.float32)
    down_part = lax.dot_general(out_grad, activated, numbers, preferred_element_type=jnp.float32)
    summed = lax.psum_scatter(
        jnp.concatenate([value_part, gate_part, down_part], axis=1) * ratio,
        "sp",
        scatter_dimension=0,
        tiled=True,
    )
    value_grad = summed[:, :local_channels]
    gate_grad = summed[:, local_channels : 2 * local_channels]
    down_grad = summed[:, 2 * local_channels :].T
    numbers = (((0,), (1,)), ((), ()))
    own = lax.dot_general(d_value, value_weight, numbers, preferred_element_type=jnp.float32)
    own = own + lax.dot_general(d_gate, gate_weight, numbers, preferred_element_type=jnp.float32)
    input_grad = lax.psum(own, "dp").astype(jnp.bfloat16)
    return (
        input_grad,
        value_grad,
        gate_grad,
        down_grad,
        kernel_grad,
        bias_grad,
        gain_grad,
        shift_grad,
    )


def solution(mesh):
    in_specs = (
        P("sp", None),
        P("sp", None),
        P(None, "dp"),
        P(None, "dp"),
        P("dp", None),
        P(None, "dp"),
        P("dp"),
        P("dp"),
        P("dp"),
    )
    out_specs = (
        P("sp", None),
        P("sp", "dp"),
        P("sp", "dp"),
        P("dp", "sp"),
        P(None, "dp"),
        P("dp"),
        P("dp"),
        P("dp"),
    )
    return jax.shard_map(
        on_device, mesh=mesh, in_specs=in_specs, out_specs=out_specs, check_vma=False
    )
```

profile of v0, /device:TPU:0, one launch (start us, length us, event | category | flops | bytes accessed | tf_op | source)
XLA Modules:
  0.0 185.2 jit_solution(6150821379646648669)
XLA Ops:
  7.2 1.2 copy-done
  8.5 1.7 convolution_convert_fusion.1
  10.9 4.9 %collective-permute-start = (f32[256,15]{0,1:T(8,128)S(1)}, f32[256,15]{0,1:T(8,128)S(1)}, u32[]{:S(2)}, u32[]{:S(2)}) collective-permute-start(f32[256,15]{0,1:T(8,128)S(1)} %get-tuple-element.71), channel_id=1, source_target_pairs={{0,4},{4,8},{8,12},{12,16},{16,20},{20,24},{24,28},{1,5},{5,9},{9,... | collective-permute-start | bytes 46088 | tf_op jit(solution)/shard_map/ppermute | solution.py:16
  15.8 1.3 collective-permute-start.1
  17.2 4.2 %collective-permute-done.1 = f32[256,15]{0,1:T(8,128)S(1)} collective-permute-done((f32[256,15]{0,1:T(8,128)S(1)}, f32[256,15]{0,1:T(8,128)S(1)}, u32[]{:S(2)}, u32[]{:S(2)}) %collective-permute-start.1) | collective-permute-done | bytes 15392 | tf_op jit(solution)/shard_map/ppermute | solution.py:19
  21.4 1.7 multiply_reduce_fusion.33
  23.2 5.7 %all-reduce.2 = (f32[320]{0:T(512)S(1)}, f32[320]{0:T(512)S(1)}) all-reduce(f32[320]{0:T(512)S(1)} %get-tuple-element.53, f32[320]{0:T(512)S(1)} %get-tuple-element.52), channel_id=1, replica_groups=mesh['sp'=8,'dp'=4] {'dp'}, use_global_device_ids=true, to_apply=%region_3.0 | all-reduce | flops 640 | bytes 5120 | tf_op jit(solution)/shard_map/psum | solution.py:57
  28.8 2.4 %multiply_reduce_fusion = (f32[256]{0:T(256)S(1)}, f32[320]{0:T(512)S(1)}, f32[320]{0:T(512)S(1)}, f32[256]{0:T(256)S(1)}, f32[256,320]{0,1:T(8,128)S(1)}) fusion(f32[256,320]{0,1:T(8,128)S(1)} %get-tuple-element.65, f32[320]{0:T(512)S(1)} %get-tuple-element.105, f32[320]{0:T(512)S(1)} %get-tuple-element.104, f32[256]{0:T(256)S(1)} %copy-done.4, ...), kind=kOutput, calls=%fused_computation.214 | convolution fusion | flops 337099648 | bytes 3023872 | tf_op jit(solution)/shard_map/dot_general | solution.py:65
  31.2 6.6 %all-reduce.1 = (f32[320]{0:T(512)S(1)}, f32[320]{0:T(512)S(1)}) all-reduce(f32[320]{0:T(512)S(1)} %get-tuple-element.47, f32[320]{0:T(512)S(1)} %get-tuple-element.48), channel_id=1, replica_groups=mesh['sp'=8,'dp'=4] {'dp'}, use_global_device_ids=true, to_apply=%region_7.0 | all-reduce | flops 640 | bytes 5120 | tf_op jit(solution)/shard_map/psum | solution.py:70
  38.4 1.3 collective-permute-start.2
  39.7 5.0 %collective-permute-start.3 = (f32[256,15]{0,1:T(8,128)S(1)}, f32[256,15]{0,1:T(8,128)S(1)}, u32[]{:S(2)}, u32[]{:S(2)}) collective-permute-start(f32[256,15]{0,1:T(8,128)S(1)} %get-tuple-element.70), channel_id=1, source_target_pairs={{0,4},{4,8},{8,12},{12,16},{16,20},{20,24},{24,28},{1,5},{5,9},{9,... | collective-permute-start | bytes 46088 | tf_op jit(solution)/shard_map/ppermute | solution.py:16
  44.7 2.2 %convolution_bitcast_fusion = f32[2048,256]{0,1:T(8,128)S(1)} fusion(bf16[320,2048]{1,0:T(8,128)(2,1)} %param.10, f32[256,320]{0,1:T(8,128)S(1)} %get-tuple-element.65, f32[256]{0:T(256)S(1)} %copy-done.6, f32[256]{0:T(256)S(1)} %copy-done.4, f32[320]{0:T(512)S(1)} %get-tuple-element.105, f32[320]{0:T(512)S(1)} %get-tuple-element.104), kind=kOutput, calls=%fused_computation.2 | convolution fusion | flops 336281600 | bytes 3740160 | tf_op jit(solution)/shard_map/dot_general | solution.py:100
  46.9 1.7 fusion.3
  48.6 0.7 convolution_bitcast_fusion.1
  49.3 0.8 convolution_bitcast_fusion.2
  50.1 3.3 %maximum_multiply_fusion = f32[2048,768]{0,1:T(8,128)} fusion(f32[2048,256]{0,1:T(8,128)S(1)} %convolution_bitcast_fusion, f32[2048,256]{0,1:T(8,128)S(1)} %convolution_bitcast_fusion.1, f32[2048,256]{0,1:T(8,128)S(1)} %convolution_bitcast_fusion.2), kind=kLoop, calls=%fused_computation | loop fusion | flops 4718592 | bytes 12582912 | tf_op jit(solution)/shard_map/mul | solution.py:102
  54.6 40.4 %all-reduce = (f32[31,256]{1,0:T(8,128)}, f32[256]{0:T(256)}, f32[256]{0:T(256)}, f32[256]{0:T(256)}) all-reduce(f32[31,256]{1,0:T(8,128)S(1)} %broadcast_multiply_fusion, f32[256]{0:T(256)S(1)} %broadcast_multiply_fusion.6, f32[256]{0:T(256)S(1)} %get-tuple-element.108, ...), channel_id=1, replica_groups=mesh['sp'=8,'dp'=4] {'sp'}, use_global_device_ids=true, to_apply=%region_41.0 | all-reduce | flops 8704 | bytes 69632 | tf_op jit(solution)/shard_map/psum | solution.py:86
  95.0 1.8 fusion.126
  96.8 2.1 %convolution_add_fusion = f32[320,2048]{1,0:T(8,128)} fusion(f32[320,2048]{1,0:T(8,128)S(1)} %fusion.126, bf16[256,320]{0,1:T(8,128)(2,1)S(1)} %get-tuple-element.63, bf16[2048,256]{1,0:T(8,128)(2,1)S(1)} %copy-done.2), kind=kOutput, calls=%fused_computation.1 | convolution fusion | flops 336199680 | bytes 6455296 | tf_op jit(solution)/shard_map/dot_general | solution.py:112
  98.9 50.2 %all-reduce.4 = bf16[320,2048]{1,0:T(8,128)(2,1)} all-reduce(f32[320,2048]{1,0:T(8,128)} %convolution_add_fusion), channel_id=1, replica_groups=mesh['sp'=8,'dp'=4] {'dp'}, use_global_device_ids=true, to_apply=%region_8.0 | all-reduce | flops 655360 | bytes 3932160 | tf_op jit(solution)/shard_map/psum | solution.py:113
  149.1 25.7 %reduce-scatter.2.cloned.1.call-done = f32[256,768]{0,1:T(8,128)} async-done(((f32[2048,768]{0,1:T(8,128)}), f32[256,768]{0,1:T(8,128)}) %reduce-scatter.2.cloned.1.call-update) | async-done | bytes 786448 | tf_op jit(solution)/shard_map/reduce_scatter | solution.py:101
  174.8 1.9 %slice_bitcast_fusion = (f32[256,256]{1,0:T(8,128)}, f32[256,256]{0,1:T(8,128)S(1)}, f32[256,256]{0,1:T(8,128)S(1)}) fusion(f32[256,768]{0,1:T(8,128)} %reduce-scatter.2.cloned.1.call-done), kind=kLoop, calls=%fused_computation.257 | loop fusion | bytes 1572864 | tf_op jit(solution)/shard_map/transpose | solution.py:109
  176.6 0.8 copy.18
  177.5 0.8 copy.17
  (34 shorter events, 2.5 us)
Async XLA Ops:
  7.2 1.3 copy-start
  7.2 3.0 %copy-start.1 = (bf16[2048,256]{1,0:T(8,128)(2,1)S(1)}, bf16[2048,256]{1,0:T(8,128)(2,1)}, u32[]{:S(2)}) copy-start(bf16[2048,256]{1,0:T(8,128)(2,1)} %param.12) | copy-start | bytes 3145732
  7.2 167.6 %reduce-scatter.2.cloned.1.call-start = ((), (), s32[]{:S(2)}) async-start(), calls=%async_computation.1 | async-start | bytes 7077888 | tf_op jit(solution)/shard_map/reduce_scatter | solution.py:101
  10.2 6.9 %copy-start.3 = (f32[31,256]{1,0:T(8,128)S(1)}, f32[31,256]{1,0:T(8,128)}, u32[]{:S(2)}) copy-start(f32[31,256]{1,0:T(8,128)} %param.14) | copy-start | bytes 95236
  10.2 11.2 %copy-start.5 = (f32[256]{0:T(256)S(1)}, f32[256]{0:T(256)}, u32[]{:S(2)}) copy-start(f32[256]{0:T(256)} %param.15) | copy-start | bytes 3076
  10.3 18.6 %copy-start.4 = (f32[256]{0:T(256)S(1)}, f32[256]{0:T(256)}, u32[]{:S(2)}) copy-start(f32[256]{0:T(256)} %param.16) | copy-start | bytes 3076
  10.3 18.6 %copy-start.6 = (f32[256]{0:T(256)S(1)}, f32[256]{0:T(256)}, u32[]{:S(2)}) copy-start(f32[256]{0:T(256)} %param.17) | copy-start | bytes 3076
  10.9 6.3 %collective-permute-start = (f32[256,15]{0,1:T(8,128)S(1)}, f32[256,15]{0,1:T(8,128)S(1)}, u32[]{:S(2)}, u32[]{:S(2)}) collective-permute-start(f32[256,15]{0,1:T(8,128)S(1)} %get-tuple-element.71), channel_id=1, source_target_pairs={{0,4},{4,8},{8,12},{12,16},{16,20},{20,24},{24,28},{1,5},{5,9},{9,... | collective-permute-start | bytes 46088 | tf_op jit(solution)/shard_map/ppermute | solution.py:16
  15.8 5.6 %collective-permute-start.1 = (f32[256,15]{0,1:T(8,128)S(1)}, f32[256,15]{0,1:T(8,128)S(1)}, u32[]{:S(2)}, u32[]{:S(2)}) collective-permute-start(f32[256,15]{0,1:T(8,128)S(1)} %get-tuple-element.72), channel_id=1, source_target_pairs={{4,0},{8,4},{12,8},{16,12},{20,16},{24,20},{28,24},{5,1},{9,5},{13... | collective-permute-start | bytes 46088 | tf_op jit(solution)/shard_map/ppermute | solution.py:19
  38.4 8.5 %collective-permute-start.2 = (f32[256,15]{0,1:T(8,128)S(1)}, f32[256,15]{0,1:T(8,128)S(1)}, u32[]{:S(2)}, u32[]{:S(2)}) collective-permute-start(f32[256,15]{0,1:T(8,128)S(1)} %get-tuple-element.69), channel_id=1, source_target_pairs={{4,0},{8,4},{12,8},{16,12},{20,16},{24,20},{28,24},{5,1},{9,5},{13... | collective-permute-start | bytes 46088 | tf_op jit(solution)/shard_map/ppermute | solution.py:19
  39.7 7.2 %collective-permute-start.3 = (f32[256,15]{0,1:T(8,128)S(1)}, f32[256,15]{0,1:T(8,128)S(1)}, u32[]{:S(2)}, u32[]{:S(2)}) collective-permute-start(f32[256,15]{0,1:T(8,128)S(1)} %get-tuple-element.70), channel_id=1, source_target_pairs={{0,4},{4,8},{8,12},{12,16},{16,20},{20,24},{24,28},{1,5},{5,9},{9,... | collective-permute-start | bytes 46088 | tf_op jit(solution)/shard_map/ppermute | solution.py:16
  54.6 42.2 %copy-start.2 = (bf16[2048,256]{1,0:T(8,128)(2,1)S(1)}, bf16[2048,256]{1,0:T(8,128)(2,1)}, u32[]{:S(2)}) copy-start(bf16[2048,256]{1,0:T(8,128)(2,1)} %param.12) | copy-start | bytes 3145732
Sparse Core Ops, SparseCore 0:
  53.5 121.1 reduce-scatter.1
where the time goes:
time: 186 us; the launch traced here: 185 us
  blocking collectives  103 us (55%)
  waiting for transfers between devices  30 us (16%)
  between operations  14.3 us (8%)
  starting transfers between devices  12.5 us (7%)
  matrix products  12.2 us (7%)
  other arithmetic  8.41 us (5%)
  local copies, waits for them, and re-layouts  4.97 us (3%)
    psum x1, blocking collectives, on_device(): input_grad = lax.psum(own, 'dp').astype(jnp.bfloat16)  50.2 us
    psum x1, blocking collectives, on_device(): lax.psum((kernel_local * ratio, jnp.sum(d_mixed, axis=1) * ratio, jnp.sum...  40.4 us
    reduce_scatter x1, waiting for transfers between devices, on_device(): lax.psum_scatter(jnp.concatenate([value_part, gate_part, down_part], axis...  25.7 us
    ppermute x2, starting transfers between devices, with_halo(): lax.ppermute(lax.slice_in_dim(block, block.shape[dim] - width, None, axis...  9.85 us
    psum x1, blocking collectives, on_device(): lax.psum((jnp.sum(d_centred, axis=0), jnp.sum(d_centred * centred, axis=0...  6.65 us
    psum x1, blocking collectives, on_device(): lax.psum((jnp.sum(mixed, axis=0), jnp.sum(mixed * mixed, axis=0)), 'dp')  5.67 us
    ppermute x2, waiting for transfers between devices, with_halo(): lax.ppermute(lax.slice_in_dim(block, 0, width, axis=dim), axis, backward)  4.21 us
  transfers between devices with their start and end apart: 5, of which 3 were waited for; matrix products, arithmetic and copies ran while one was open for 4% of the time, Pallas kernels for 0%

commit v1 on v0

v1 whole, which is shorter than its diff:
```python
import functools
import math

import jax
import jax.numpy as jnp
from jax import lax
from jax.experimental import pallas as pl
from jax.experimental.pallas import tpu as pltpu
from jax.sharding import PartitionSpec as P

EPS = 1e-05
F32 = jnp.float32
BF16 = jnp.bfloat16
MESH = pl.DeviceIdType.MESH
NT = (((1,), (1,)), ((), ()))
TN = (((0,), (0,)), ((), ()))
EXACT = lax.Precision.HIGHEST
PAD = 16
ROWS = 32


def dot(a, b, numbers, precision=None):
    return lax.dot_general(a, b, numbers, precision=precision, preferred_element_type=F32)


def kernel(
    sp,
    dp,
    ratio,
    x,
    og,
    wv,
    wg,
    wd,
    ck,
    bias,
    gain,
    shift,
    ig_out,
    vg_out,
    gg_out,
    dg_out,
    small_out,
    value,
    opening,
    glu,
    mixed,
    d_act,
    d_pad,
    act,
    dv,
    dg,
    cols,
    stats,
    stats2,
    part,
    ring_src,
    ring_dst,
    ig_send,
    ig_recv,
    ig_own,
    ig_sum,
    ig_peer,
    small,
    small_recv,
    halo_send,
    halo_recv,
    stat_send,
    stat_recv,
    ring_send,
    ring_recv,
    ig_ssem,
    ig_rsem,
    small_ssem,
    small_rsem,
):
    tokens, width = x.shape
    taps, chans = ck.shape
    channels = chans * dp
    reach = taps // 2
    chunk = width // sp
    half_chunk = chunk // 2
    tile = min(256, width)
    s = lax.axis_index("sp")
    d = lax.axis_index("dp")
    bits_sp = sp.bit_length() - 1
    bits_dp = dp.bit_length() - 1

    def flip(i, bit):
        step = 1 << bit
        return i + step * (1 - 2 * lax.rem(lax.div(i, step), 2))

    def index_of(p):
        far = lax.div(p, sp // 2)
        return (1 - far) * 2 * p + far * (2 * sp - 1 - 2 * p)

    odd = lax.rem(s, 2)
    pos = (1 - odd) * lax.div(s, 2) + odd * (sp - 1 - lax.div(s, 2))
    ahead = index_of(lax.rem(pos + 1, sp))
    behind = index_of(lax.rem(pos + sp - 1, sp))

    barrier = pltpu.get_barrier_semaphore()
    peers = [ahead, behind, lax.rem(s + 1, sp), lax.rem(s + sp - 1, sp)]
    peers += [flip(s, bit) for bit in range(bits_sp)]
    for peer in peers:
        pl.semaphore_signal(barrier, inc=1, device_id={"sp": peer}, device_id_type=MESH)
    for off in range(1, dp):
        pl.semaphore_signal(
            barrier, inc=1, device_id={"dp": lax.rem(d + off, dp)}, device_id_type=MESH
        )

    numbers = (((1,), (0,)), ((), ()))
    value[...] = dot(x[...], wv[...], numbers).astype(BF16).astype(F32)
    opening[...] = dot(x[...], wg[...], numbers).astype(BF16).astype(F32)

    def row_loop(fn, init=None, rows=ROWS):
        def step(i, carry):
            return fn(pl.multiple_of(i * rows, rows), carry)

        return lax.fori_loop(0, tokens // rows, step, init)

    def make_glu(r, _):
        here = pl.ds(r, ROWS)
        o = jax.nn.sigmoid(opening[here, :])
        opening[here, :] = o
        glu[pl.ds(r + PAD, ROWS), :] = value[here, :] * o

    row_loop(make_glu)
    pl.semaphore_wait(barrier, len(peers) + dp - 1)

    has_low, has_high = s > 0, s < sp - 1

    def halo_copies(buf, at):
        up = pltpu.make_async_remote_copy(
            src_ref=buf.at[pl.ds(tokens, PAD)],
            dst_ref=buf.at[pl.ds(0, PAD)],
            send_sem=halo_send.at[at],
            recv_sem=halo_recv.at[at],
            device_id={"sp": lax.rem(s + 1, sp)},
            device_id_type=MESH,
        )
        down = pltpu.make_async_remote_copy(
            src_ref=buf.at[pl.ds(PAD, PAD)],
            dst_ref=buf.at[pl.ds(tokens + PAD, PAD)],
            send_sem=halo_send.at[at + 1],
            recv_sem=halo_recv.at[at + 1],
            device_id={"sp": lax.rem(s + sp - 1, sp)},
            device_id_type=MESH,
        )
        return up, down

    def halo_start(buf, at):
        up, down = halo_copies(buf, at)
        pl.when(has_high)(up.start)
        pl.when(has_low)(down.start)

        @pl.when(s == 0)
        def _():
            buf[pl.ds(0, PAD), :] = jnp.zeros((PAD, chans), F32)

        @pl.when(s == sp - 1)
        def _():
            buf[pl.ds(tokens + PAD, PAD), :] = jnp.zeros((PAD, chans), F32)

    def halo_wait(buf, at):
        up, down = halo_copies(buf, at)

        @pl.when(has_low)
        def _():
            up.wait_recv()
            down.wait_send()

        @pl.when(has_high)
        def _():
            down.wait_recv()
            up.wait_send()

    halo_start(glu, 0)
    d_act[...] = dot(og[...], wd[...], NT)
    halo_wait(glu, 0)

    span = ROWS + 2 * PAD

    def shifted(buf, r, offset):
        window = buf[pl.ds(r, span), :]
        return pltpu.roll(window, span - offset, 0) if offset else window

    def slide(buf, r, offset_of, acc):
        for low in range(8):
            those = [tap for tap in range(taps) if offset_of(tap) % 8 == low]
            if those:
                window = shifted(buf, r, low)
                for tap in those:
                    high = offset_of(tap) - low
                    acc = acc + ck[tap : tap + 1, :] * window[high : high + ROWS]
        return acc

    def conv(r, _):
        acc = jnp.zeros((ROWS, chans), F32) + bias[...]
        mixed[pl.ds(r, ROWS), :] = slide(glu, r, lambda tap: tap + PAD - reach, acc)

    row_loop(conv)

    ones = jnp.ones((8, chans), F32)
    line = lax.broadcasted_iota(jnp.int32, (8, tokens), 0)
    eye = (
        lax.broadcasted_iota(jnp.int32, (8, 128), 0)
        == lax.broadcasted_iota(jnp.int32, (8, 128), 1)
    ).astype(F32)

    def stat_copy(buf, off, at):
        return pltpu.make_async_remote_copy(
            src_ref=buf.at[0],
            dst_ref=buf.at[off],
            send_sem=stat_send.at[at * dp + off],
            recv_sem=stat_recv.at[at * dp + off],
            device_id={"dp": lax.rem(d + off, dp)},
            device_id_type=MESH,
        )

    def stat_start(buf, at, one, two):
        buf[0] = jnp.where(line == 0, dot(ones, one, NT, EXACT), dot(ones, two, NT, EXACT))
        for off in range(1, dp):
            stat_copy(buf, off, at).start()

    def stat_wait(buf, at):
        for off in range(1, dp):
            stat_copy(buf, off, at).wait()
        total = buf[0]
        for off in range(1, dp):
            total = total + buf[off]
        return total * (1.0 / channels)

    stat_start(stats, 0, mixed[...], mixed[...] * mixed[...])
    moments = stat_wait(stats, 0)
    mean = moments[0:1]
    inv = lax.rsqrt(moments[1:2] - mean * mean + EPS)
    cols[0] = dot(jnp.where(line == 0, mean, inv), eye, TN, EXACT)

    def norm(r, carry):
        gain_sum, shift_sum = carry
        here = pl.ds(r, ROWS)
        col = cols[0, here, :]
        centred = (mixed[here, :] - col[:, 0:1]) * col[:, 1:2]
        normed = centred * gain[...] + shift[...]
        sig = jax.nn.sigmoid(normed)
        act[here, :] = (normed * sig).astype(BF16)
        d_normed = d_act[here, :] * sig * (1.0 + normed * (1.0 - sig))
        mixed[here, :] = centred
        d_act[here, :] = d_normed * gain[...]
        gain_sum = gain_sum + jnp.sum(d_normed * centred, axis=0, keepdims=True)
        shift_sum = shift_sum + jnp.sum(d_normed, axis=0, keepdims=True)
        return gain_sum, shift_sum

    zero = jnp.zeros((1, chans), F32)
    gain_sum, shift_sum = row_loop(norm, (zero, zero))
    stat_start(stats2, 1, d_act[...], d_act[...] * mixed[...])

    def weight_grad(at, rows, factor):
        def step(i, _):
            here = pl.ds(pl.multiple_of(i * tile, tile), tile)
            part[at, here, :] = dot(rows[:, here], factor[...], TN) * ratio

        lax.fori_loop(0, width // tile, step, None)

    streams = [(0, 0, 1), (1, 0, -1), (0, 1, 1), (1, 1, -1), (2, 0, 1), (2, 1, -1)]
    late, early = (0, 1, 2, 3), (4, 5)

    def piece(stream, p):
        at, half, _ = streams[stream]
        first = index_of(lax.rem(p + 2 * sp, sp)) * chunk + half * half_chunk
        return part[at, pl.ds(pl.multiple_of(first, half_chunk), half_chunk), :]

    def ring_copy(stream, k):
        return pltpu.make_async_remote_copy(
            src_ref=ring_src.at[stream, k],
            dst_ref=ring_dst.at[stream, k],
            send_sem=ring_send.at[stream, k],
            recv_sem=ring_recv.at[stream, k],
            device_id={"sp": ahead if streams[stream][2] == 1 else behind},
            device_id_type=MESH,
        )

    def ring_step(k, which):
        for stream in which:
            way = streams[stream][2]
            mine = piece(stream, pos - way * (1 + k))
            if not (isinstance(k, int) and k == 0):
                ring_copy(stream, k - 1).wait_recv()
                mine = mine + ring_dst[stream, k - 1].astype(F32)
            ring_src[stream, k] = mine.astype(BF16)
            ring_copy(stream, k).start()

    def ring_end(which, outs):
        for stream in which:
            at, half, _ = streams[stream]
            ring_copy(stream, sp - 2).wait_recv()
            outs[at][pl.ds(half * half_chunk, half_chunk), :] = piece(stream, pos) + ring_dst[
                stream, sp - 2
            ].astype(F32)

    weight_grad(2, og, act)
    ring_step(0, early)

    moments = stat_wait(stats2, 1)
    cols[1] = dot(moments, eye, TN, EXACT)

    def norm_back(r, bias_sum):
        here = pl.ds(r, ROWS)
        col, back = cols[0, here, :], cols[1, here, :]
        d_mixed = col[:, 1:2] * (d_act[here, :] - back[:, 0:1] - mixed[here, :] * back[:, 1:2])
        d_pad[pl.ds(r + PAD, ROWS), :] = d_mixed
        return bias_sum + jnp.sum(d_mixed, axis=0, keepdims=True)

    bias_sum = row_loop(norm_back, zero)
    halo_start(d_pad, 2)

    small[0] = jnp.zeros(small.shape[1:], F32)
    for low in range(0, 8, 2):
        those = [
            [tap for tap in range(taps) if (tap + PAD - reach) % 8 == low + at] for at in range(2)
        ]

        def taps_sum(r, sums, low=low, those=those):
            grad = d_pad[pl.ds(r + PAD, ROWS), :]
            new = []
            for at in range(2):
                window = shifted(glu, r, low + at)
                for tap in those[at]:
                    high = tap + PAD - reach - low - at
                    prod = grad * window[high : high + ROWS]
                    acc = sums[len(new)]
                    for row in range(0, ROWS, 8):
                        acc = acc + prod[row : row + 8]
                    new.append(acc)
            return tuple(new)

        flat = those[0] + those[1]
        sums = row_loop(taps_sum, tuple(jnp.zeros((8, chans), F32) for _ in flat))
        for acc, tap in zip(sums, flat):
            small[0, tap : tap + 1, :] = jnp.sum(acc, axis=0, keepdims=True) * ratio
        if low == 2:
            ring_step(1, early)
    small[0, taps : taps + 1, :] = bias_sum * ratio
    small[0, taps + 1 : taps + 2, :] = gain_sum * ratio
    small[0, taps + 2 : taps + 3, :] = shift_sum * ratio

    def small_copy(bit):
        return pltpu.make_async_remote_copy(
            src_ref=small.at[bit],
            dst_ref=small_recv.at[bit],
            send_sem=small_ssem.at[bit],
            recv_sem=small_rsem.at[bit],
            device_id={"sp": flip(s, bit)},
            device_id_type=MESH,
        )

    def small_next(bit):
        small_copy(bit).wait_recv()
        return small[bit] + small_recv[bit]

    halo_wait(d_pad, 2)
    small_copy(0).start()

    def conv_back(r, _):
        here = pl.ds(r, ROWS)
        acc = jnp.zeros((ROWS, chans), F32)
        acc = slide(d_pad, r, lambda tap: PAD + reach - tap, acc)
        o = opening[here, :]
        grad = acc * o
        dv[here, :] = grad.astype(BF16)
        dg[here, :] = (grad * value[here, :] * (1.0 - o)).astype(BF16)

    row_loop(conv_back)
    weight_grad(0, x, dv)
    ring_step(0, late[0::2])
    weight_grad(1, x, dg)
    ring_step(0, late[1::2])
    ring_step(2, early)

    half = tokens // 2
    mine = pl.multiple_of(lax.rem(d, 2) * half, half)
    other = pl.multiple_of((1 - lax.rem(d, 2)) * half, half)

    def input_grad(first, target):
        def step(i, _):
            here = pl.ds(pl.multiple_of(i * tile, tile), tile)
            rows = pl.ds(first, half)
            got = dot(dv[rows, :], wv[here, :], NT) + dot(dg[rows, :], wg[here, :], NT)
            target[:, here] = got.astype(target.dtype)

        lax.fori_loop(0, width // tile, step, None)

    def ig_copy(at, src, dst, bit):
        return pltpu.make_async_remote_copy(
            src_ref=src,
            dst_ref=dst,
            send_sem=ig_ssem.at[at],
            recv_sem=ig_rsem.at[at],
            device_id={"dp": flip(d, bit)},
            device_id_type=MESH,
        )

    input_grad(other, ig_send)
    copy0 = ig_copy(0, ig_send, ig_recv, 0)
    copy0.start()
    input_grad(mine, ig_own)
    copy0.wait_recv()

    def wide_loop(fn):
        def step(i, _):
            fn(pl.ds(pl.multiple_of(i * tile, tile), tile))

        lax.fori_loop(0, width // tile, step, None)

    def pair_sum(here):
        ig_sum[0, :, here] = (ig_own[:, here] + ig_recv[:, here].astype(F32)).astype(BF16)

    def y_copy(bit):
        return ig_copy(bit, ig_sum.at[bit - 1], ig_peer.at[bit - 1], bit)

    wide_loop(pair_sum)
    last = bits_dp
    if last > 1:
        y_copy(1).start()
    small[1] = small_next(0)
    if bits_sp > 1:
        small_copy(1).start()

    everything = late + early
    ring_step(1, late)
    ring_step(3, early) if sp > 4 else None
    ring_step(2, late)
    for bit in range(1, bits_sp):
        small[bit + 1] = small_next(bit)
        if bit + 1 < bits_sp:
            small_copy(bit + 1).start()
    ring_step(3, late)

    for_early = 4

    def both(k, _):
        ring_step(k, everything)

    lax.fori_loop(for_early, sp - 2, both, None)

    for bit in range(1, bits_dp):
        y_copy(bit).wait_recv()

        def add(here, bit=bit):
            got = ig_sum[bit - 1, :, here].astype(F32) + ig_peer[bit - 1, :, here].astype(F32)
            ig_sum[bit, :, here] = got.astype(BF16)

        wide_loop(add)
        if bit + 1 < bits_dp:
            y_copy(bit + 1).start()

    final = bits_dp - 1
    give = ig_copy(
        bits_dp, ig_sum.at[final], ig_out.at[pl.ds(mine, half)], 0
    )
    give.start()
    ring_step(sp - 2, everything)

    def keep(here):
        ig_out[pl.ds(mine, half), here] = ig_sum[final, :, here]

    wide_loop(keep)
    small_out[...] = small[bits_sp]
    outs = (vg_out, gg_out, dg_out)
    ring_end(everything, outs)

    copy0.wait_send()
    for bit in range(1, bits_dp):
        y_copy(bit).wait_send()
    give.wait()
    for bit in range(bits_sp):
        small_copy(bit).wait_send()

    def drain(k, _):
        for stream in everything:
            ring_copy(stream, k).wait_send()

    lax.fori_loop(0, sp - 1, drain, None)


def on_device(
    normed_input,
    out_grad,
    value_weight,
    gate_weight,
    down_weight,
    conv_kernel,
    conv_bias,
    norm_gain,
    norm_shift,
):
    tokens, width = normed_input.shape
    taps, chans = conv_kernel.shape
    sp, dp = lax.axis_size("sp"), lax.axis_size("dp")
    ratio = 1.0 / math.sqrt(tokens * sp)
    chunk = width // sp
    bits_sp, bits_dp = sp.bit_length() - 1, dp.bit_length() - 1
    small_rows = -(-(taps + 3) // 8) * 8
    half = tokens // 2
    full = (tokens, chans)
    vmem = pl.BlockSpec(memory_space=pltpu.VMEM)
    dma = pltpu.SemaphoreType.DMA
    ig, vg, gg, dgrad, small = pl.pallas_call(
        functools.partial(kernel, sp, dp, ratio),
        out_shape=(
            jax.ShapeDtypeStruct((tokens, width), BF16),
            jax.ShapeDtypeStruct((chunk, chans), F32),
            jax.ShapeDtypeStruct((chunk, chans), F32),
            jax.ShapeDtypeStruct((chunk, chans), F32),
            jax.ShapeDtypeStruct((small_rows, chans), F32),
        ),
        in_specs=[vmem] * 9,
        out_specs=(vmem,) * 5,
        scratch_shapes=[
            pltpu.VMEM(full, F32),
            pltpu.VMEM(full, F32),
            pltpu.VMEM((tokens + 2 * PAD, chans), F32),
            pltpu.VMEM(full, F32),
            pltpu.VMEM(full, F32),
            pltpu.VMEM((tokens + 2 * PAD, chans), F32),
            pltpu.VMEM(full, BF16),
            pltpu.VMEM(full, BF16),
            pltpu.VMEM(full, BF16),
            pltpu.VMEM((2, tokens, 128), F32),
            pltpu.VMEM((dp, 8, tokens), F32),
            pltpu.VMEM((dp, 8, tokens), F32),
            pltpu.VMEM((3, width, chans), F32),
            pltpu.VMEM((6, sp - 1, chunk // 2, chans), BF16),
            pltpu.VMEM((6, sp - 1, chunk // 2, chans), BF16),
            pltpu.VMEM((half, width), BF16),
            pltpu.VMEM((half, width), BF16),
            pltpu.VMEM((half, width), F32),
            pltpu.VMEM((bits_dp, half, width), BF16),
            pltpu.VMEM((bits_dp - 1, half, width), BF16),
            pltpu.VMEM((bits_sp + 1, small_rows, chans), F32),
            pltpu.VMEM((bits_sp, small_rows, chans), F32),
            dma((4,)),
            dma((4,)),
            dma((2 * dp,)),
            dma((2 * dp,)),
            dma((6, sp - 1)),
            dma((6, sp - 1)),
            dma((bits_dp + 1,)),
            dma((bits_dp + 1,)),
            dma((bits_sp,)),
            dma((bits_sp,)),
        ],
        compiler_params=pltpu.CompilerParams(
            collective_id=0, has_side_effects=True, vmem_limit_bytes=60 * 1024 * 1024
        ),
    )(
        normed_input,
        out_grad,
        value_weight,
        gate_weight,
        down_weight,
        conv_kernel,
        conv_bias[None, :],
        norm_gain[None, :],
        norm_shift[None, :],
    )
    return (
        ig,
        vg,
        gg,
        dgrad.T,
        small[:taps],
        small[taps],
        small[taps + 1],
        small[taps + 2],
    )


def solution(mesh):
    in_specs = (
        P("sp", None),
        P("sp", None),
        P(None, "dp"),
        P(None, "dp"),
        P("dp", None),
        P(None, "dp"),
        P("dp"),
        P("dp"),
        P("dp"),
    )
    out_specs = (
        P("sp", None),
        P("sp", "dp"),
        P("sp", "dp"),
        P("dp", "sp"),
        P(None, "dp"),
        P("dp"),
        P("dp"),
        P("dp"),
    )
    return jax.shard_map(
        on_device, mesh=mesh, in_specs=in_specs, out_specs=out_specs, check_vma=False
    )
```

time: 186 us -> 75.8 us (0.41)
  blocking collectives: 103 us -> 0 us
  Pallas kernels: 0 us -> 66.3 us
  waiting for transfers between devices: 30 us -> 0 us
  between operations: 14.3 us -> 0.65 us
  starting transfers between devices: 12.5 us -> 0 us
  matrix products: 12.2 us -> 0 us
  other arithmetic: 8.41 us -> 0 us
  local copies, waits for them, and re-layouts: 4.97 us -> 8.5 us
    psum x4 -> x0, blocking collectives: 103 us -> none  [the longest x1 50.2 us: on_device(): input_grad = lax.psum(own, 'dp').astype(jnp.bfloat16)]
    pallas_call x0 -> x1, Pallas kernels: none -> 66.3 us  [on_device(): pl.pallas_call(functools.partial(kernel, sp, dp, ratio), out_shape=(jax.S...]
    reduce_scatter x1 -> x0, waiting for transfers between devices: 25.7 us -> none  [on_device(): lax.psum_scatter(jnp.concatenate([value_part, gate_part, down_part], axis...]
    ppermute x4 -> x0, starting transfers between devices: 12.4 us -> none  [the longest x2 9.85 us: with_halo(): lax.ppermute(lax.slice_in_dim(block, block.shape[dim] - width, None, axis...]
    dot_general x8 -> x0, matrix products: 12.2 us -> none  [the longest x1 2.37 us: on_device(): lax.dot_general(down_weight, out_grad, (((1,), (1,)), ((), ())), preferre...]
    ppermute x4 -> x0, waiting for transfers between devices: 4.28 us -> none  [the longest x2 4.21 us: with_halo(): lax.ppermute(lax.slice_in_dim(block, 0, width, axis=dim), axis, backward)]
    mul x5 -> x0, other arithmetic: 3.38 us -> none  [the longest x1 3.27 us: on_device(): jnp.concatenate([value_part, gate_part, down_part], axis=1) * ratio]
    reduce_sum x5 -> x0, other arithmetic: 3.28 us -> none  [the longest x1 1.71 us: on_device(): jnp.sum(mixed * mixed, axis=0)]
  transfers between devices with their start and end apart: 5 -> 0, of which waited for: 3 -> 0; matrix products, arithmetic and copies ran while one was open for 4% -> 0% of each run, Pallas kernels for 0% -> 0%
where the time goes in v1:
time: 75.8 us; the launch traced here: 75.5 us
  Pallas kernels  66.3 us (87%)
  local copies, waits for them, and re-layouts  8.5 us (11%)
    pallas_call x1, Pallas kernels, on_device(): pl.pallas_call(functools.partial(kernel, sp, dp, ratio), out_shape=(jax.S...  66.3 us
    unnamed x8, local copies, waits for them, and re-layouts  5.77 us

profile of v1, /device:TPU:0, one launch (start us, length us, event | category | flops | bytes accessed | tf_op | source)
XLA Modules:
  0.0 75.5 jit_solution(3134779084303211377)
XLA Ops:
  0.6 66.3 %shard_map.152 = (bf16[320,2048]{1,0:T(8,128)(2,1)}, f32[256,256]{1,0:T(8,128)}, f32[256,256]{1,0:T(8,128)}, f32[256,256]{1,0:T(8,128)}, f32[40,256]{1,0:T(8,128)}) custom-call(bf16[320,2048]{1,0:T(8,128)(2,1)} %x.1, bf16[320,2048]{1,0:T(8,128)(2,1)} %og.1, bf16[2048,256]{1,0:T(8,128)(2,1)} %wv.1, bf16[2048,256]{1,0:T(8,128)(2,1)} %wg.1, ...), custom_call_target="tpu_custom_call" | custom-call | tf_op jit(solution)/shard_map/pallas_call | solution.py:509
  67.0 1.3 %fusion = (f32[1,256]{1,0:T(1,128)}, f32[1,256]{1,0:T(1,128)}, f32[1,256]{1,0:T(1,128)}) fusion(f32[40,256]{1,0:T(8,128)} %get-tuple-element.17), kind=kLoop, calls=%fused_computation | loop fusion | bytes 6144 | tf_op jit(solution)/shard_map/slice | solution.py:576
  68.3 1.4 %slice.12 = f32[31,256]{1,0:T(8,128)} slice(f32[40,256]{1,0:T(8,128)} %get-tuple-element.17), slice={[0:31], [0:256]} | slice | bytes 63488 | tf_op jit(solution)/shard_map/slice | solution.py:573
  69.7 1.8 %copy.17 = f32[256,256]{1,0:T(8,128)} copy(f32[256,256]{0,1:T(8,128)} %bitcast.7) | data formatting | bytes 524288
  71.5 0.0 copy-start.1
  71.5 0.0 copy-start
  71.5 2.6 %copy.21 = bf16[320,2048]{1,0:T(8,128)(2,1)} copy(bf16[320,2048]{1,0:T(8,128)(2,1)} %get-tuple-element.37) | data formatting | bytes 2621440
  74.1 0.0 copy-done.1
  74.1 0.7 copy.22
  74.8 0.0 copy-done
  74.8 0.7 copy.23
Async XLA Ops:
  71.5 2.6 %copy-start.1 = (f32[256,256]{1,0:T(8,128)S(1)}, f32[256,256]{1,0:T(8,128)}, u32[]{:S(2)}) copy-start(f32[256,256]{1,0:T(8,128)} %get-tuple-element.38) | copy-start | bytes 786436
  71.5 3.3 %copy-start = (f32[256,256]{1,0:T(8,128)S(1)}, f32[256,256]{1,0:T(8,128)}, u32[]{:S(2)}) copy-start(f32[256,256]{1,0:T(8,128)} %get-tuple-element.39) | copy-start | bytes 786436

commit v2 on v1

--- a/solution.py
+++ b/solution.py
@@ -17,6 +17,8 @@
 EXACT = lax.Precision.HIGHEST
 PAD = 16
 ROWS = 32
+MAIN = 61_900_000
+FINISH = 16_000_000
 
 
 def dot(a, b, numbers, precision=None):
@@ -27,11 +29,11 @@
     sp,
     dp,
     ratio,
-    x,
-    og,
-    wv,
-    wg,
-    wd,
+    x_hbm,
+    og_hbm,
+    wv_hbm,
+    wg_hbm,
+    wd_hbm,
     ck,
     bias,
     gain,
@@ -41,6 +43,12 @@
     gg_out,
     dg_out,
     small_out,
+    x,
+    og,
+    wv,
+    wg,
+    wd,
+    load_sem,
     value,
     opening,
     glu,
@@ -99,6 +107,15 @@
     ahead = index_of(lax.rem(pos + 1, sp))
     behind = index_of(lax.rem(pos + sp - 1, sp))
 
+    loads = [
+        pltpu.make_async_copy(src, dst, load_sem.at[at])
+        for at, (src, dst) in enumerate(
+            [(x_hbm, x), (wv_hbm, wv), (wg_hbm, wg), (og_hbm, og), (wd_hbm, wd)]
+        )
+    ]
+    for load in loads:
+        load.start()
+
     barrier = pltpu.get_barrier_semaphore()
     peers = [ahead, behind, lax.rem(s + 1, sp), lax.rem(s + sp - 1, sp)]
     peers += [flip(s, bit) for bit in range(bits_sp)]
@@ -110,7 +127,10 @@
         )
 
     numbers = (((1,), (0,)), ((), ()))
+    loads[0].wait()
+    loads[1].wait()
     value[...] = dot(x[...], wv[...], numbers).astype(BF16).astype(F32)
+    loads[2].wait()
     opening[...] = dot(x[...], wg[...], numbers).astype(BF16).astype(F32)
 
     def row_loop(fn, init=None, rows=ROWS):
@@ -176,6 +196,8 @@
             up.wait_send()
 
     halo_start(glu, 0)
+    loads[3].wait()
+    loads[4].wait()
     d_act[...] = dot(og[...], wd[...], NT)
     halo_wait(glu, 0)
 
@@ -482,6 +504,22 @@
             ring_copy(stream, k).wait_send()
 
     lax.fori_loop(0, sp - 1, drain, None)
+
+
+def finish(ig, vg, gg, dgrad, small, ig_o, vg_o, gg_o, dg_o, k_o, b_o, g_o, s_o, sem):
+    copies = [
+        pltpu.make_async_copy(src, dst, sem.at[at])
+        for at, (src, dst) in enumerate([(ig, ig_o), (vg, vg_o), (gg, gg_o)])
+    ]
+    for copy in copies:
+        copy.start()
+    taps = k_o.shape[0]
+    dg_o[...] = dgrad[...].T
+    k_o[...] = small[0:taps, :]
+    for at, out in enumerate((b_o, g_o, s_o)):
+        out[...] = small[taps + at, :]
+    for copy in copies:
+        copy.wait()
 
 
 def on_device(
@@ -505,19 +543,26 @@
     half = tokens // 2
     full = (tokens, chans)
     vmem = pl.BlockSpec(memory_space=pltpu.VMEM)
+    hbm = pl.BlockSpec(memory_space=pltpu.HBM)
     dma = pltpu.SemaphoreType.DMA
     ig, vg, gg, dgrad, small = pl.pallas_call(
         functools.partial(kernel, sp, dp, ratio),
         out_shape=(
-            jax.ShapeDtypeStruct((tokens, width), BF16),
-            jax.ShapeDtypeStruct((chunk, chans), F32),
-            jax.ShapeDtypeStruct((chunk, chans), F32),
-            jax.ShapeDtypeStruct((chunk, chans), F32),
-            jax.ShapeDtypeStruct((small_rows, chans), F32),
+            pltpu.VMEM((tokens, width), BF16),
+            pltpu.VMEM((chunk, chans), F32),
+            pltpu.VMEM((chunk, chans), F32),
+            pltpu.VMEM((chunk, chans), F32),
+            pltpu.VMEM((small_rows, chans), F32),
         ),
-        in_specs=[vmem] * 9,
+        in_specs=[hbm] * 5 + [vmem] * 4,
         out_specs=(vmem,) * 5,
         scratch_shapes=[
+            pltpu.VMEM((tokens, width), BF16),
+            pltpu.VMEM((tokens, width), BF16),
+            pltpu.VMEM((width, chans), BF16),
+            pltpu.VMEM((width, chans), BF16),
+            pltpu.VMEM((chans, width), BF16),
+            dma((5,)),
             pltpu.VMEM(full, F32),
             pltpu.VMEM(full, F32),
             pltpu.VMEM((tokens + 2 * PAD, chans), F32),
@@ -552,7 +597,7 @@
             dma((bits_sp,)),
         ],
         compiler_params=pltpu.CompilerParams(
-            collective_id=0, has_side_effects=True, vmem_limit_bytes=60 * 1024 * 1024
+            collective_id=0, has_side_effects=True, vmem_limit_bytes=MAIN
         ),
     )(
         normed_input,
@@ -565,16 +610,24 @@
         norm_gain[None, :],
         norm_shift[None, :],
     )
-    return (
-        ig,
-        vg,
-        gg,
-        dgrad.T,
-        small[:taps],
-        small[taps],
-        small[taps + 1],
-        small[taps + 2],
-    )
+    row = jax.ShapeDtypeStruct((chans,), F32)
+    return pl.pallas_call(
+        finish,
+        out_shape=(
+            jax.ShapeDtypeStruct(ig.shape, BF16),
+            jax.ShapeDtypeStruct(vg.shape, F32),
+            jax.ShapeDtypeStruct(gg.shape, F32),
+            jax.ShapeDtypeStruct((chans, chunk), F32),
+            jax.ShapeDtypeStruct((taps, chans), F32),
+            row,
+            row,
+            row,
+        ),
+        in_specs=[vmem] * 5,
+        out_specs=(hbm,) * 3 + (vmem,) * 5,
+        scratch_shapes=[dma((3,))],
+        compiler_params=pltpu.CompilerParams(vmem_limit_bytes=FINISH),
+    )(ig, vg, gg, dgrad, small)
 
 
 def solution(mesh):

time: 75.8 us -> 67.7 us (0.89)
  local copies, waits for them, and re-layouts: 8.5 us -> 0 us
    unnamed x8 -> x0, local copies, waits for them, and re-layouts: 5.77 us -> none
    slice x2 -> x0, local copies, waits for them, and re-layouts: 2.72 us -> none  [the longest x1 1.37 us: on_device(): small[:taps]]
    pallas_call x1 -> x2, Pallas kernels: 66.3 us -> 66.8 us  [the longest x1 64.9 us: on_device(): pl.pallas_call(functools.partial(kernel, sp, dp, ratio), out_shape=(pltpu...]
where the time goes in v2:
time: 67.7 us; the launch traced here: 67.5 us
  Pallas kernels  66.8 us (99%)
    pallas_call x1, Pallas kernels, on_device(): pl.pallas_call(functools.partial(kernel, sp, dp, ratio), out_shape=(pltpu...  64.9 us
    pallas_call x1, Pallas kernels, on_device(): pl.pallas_call(finish, out_shape=(jax.ShapeDtypeStruct(ig.shape, BF16), j...  1.98 us

profile of v2, /device:TPU:0, one launch (start us, length us, event | category | flops | bytes accessed | tf_op | source)
XLA Modules:
  0.0 67.5 jit_solution(11890046101101131748)
XLA Ops:
  0.6 64.9 %shard_map.152 = (bf16[320,2048]{1,0:T(8,128)(2,1)S(1)}, f32[256,256]{1,0:T(8,128)S(1)}, f32[256,256]{1,0:T(8,128)S(1)}, f32[256,256]{1,0:T(8,128)S(1)}, f32[40,256]{1,0:T(8,128)S(1)}) custom-call(bf16[320,2048]{1,0:T(8,128)(2,1)} %x_hbm.1, bf16[320,2048]{1,0:T(8,128)(2,1)} %og_hbm.1, bf16[2048,256]{1,0:T(8,128)(2,1)} %wv_hbm.1, bf16[2048,256]{1,0:T(8,128)(2,1)} %wg_hbm.1, ...), custom_call_target="tpu_custom_call" | custom-call | tf_op jit(solution)/shard_map/pallas_call | solution.py:548
  65.5 2.0 %shard_map.153 = (bf16[320,2048]{1,0:T(8,128)(2,1)}, f32[256,256]{1,0:T(8,128)}, f32[256,256]{1,0:T(8,128)}, f32[256,256]{1,0:T(8,128)}, f32[31,256]{1,0:T(8,128...) custom-call(bf16[320,2048]{1,0:T(8,128)(2,1)S(1)} %get-tuple-element.13.ig, f32[256,256]{1,0:T(8,128)S(1)} %get-tuple-element.14.vg, ...), custom_call_target="tpu_custom_call" | custom-call | tf_op jit(solution)/shard_map/pallas_call | solution.py:614
